TPU v7x, 32 devices: a whole 2x2x4 slice. The times are simulated.
32 devices in a mesh: sp: 8 (over z, x), tp: 4 (over y, core).
Axes of the slice: x: 2, y: 2, z: 4, core: 2. Of those that a mesh axis runs over, the one named last changes fastest.
Arguments:
- conv_in: bfloat16 [6144, 1024], P('sp', 'tp'), may hold values from -6 to 6
- conv_pre: bfloat16 [6144, 1024], P('sp', 'tp'), may hold values from -6 to 6
- conv_post: bfloat16 [6144, 1024], P('sp', 'tp'), may hold values from -6 to 6
- taps: float32 [3, 1024], P(None, 'tp'), may hold values from -3 to 3
- out_proj: bfloat16 [1024, 2048], P('tp'), may hold values from -0.1875 to 0.1875
- stream: bfloat16 [6144, 2048], P(('sp', 'tp')), may hold values from -6 to 6
- norm_gain: float32 [2048], replicated, may hold values from 0.1 to 1.9
- routes: int32 [6144, 2], P(('sp', 'tp')), may hold values from 0 to 7, all different within a row; in each aligned block of 192 rows (0 to 191, 192 to 383, ...) at most 64 rows name the same one
- route_weight: float32 [6144, 2], P(('sp', 'tp')), may hold values from 0.1 to 1
- gate_w: bfloat16 [8, 2048, 2048], P('sp', None, 'tp'), may hold values from -0.52734375 to 0.52734375
- up_w: bfloat16 [8, 2048, 2048], P('sp', None, 'tp'), may hold values from -0.52734375 to 0.52734375
- down_w: bfloat16 [8, 2048, 2048], P('sp', 'tp'), may hold values from -0.013244629 to 0.013244629
Outputs:
- output: bfloat16 [6144, 2048], P(('sp', 'tp'))
Inputs may be any that keep to these rules, and one draw needn't show every extreme that they name: `routes`: each row names 2 different experts. In each aligned block of 192 rows no expert is named more than 64 times, a bound that some block reaches.
All inputs are finite; a program needn't handle non-finite values.
Results may differ from a plain program's by a relative error of at most 0.015.
Values may be sent and summed in bfloat16 or wider, within the bound.
A program may use at most 128 MiB of HBM per device.

v0:
```python
import jax
import jax.numpy as jnp
from jax import lax
from jax.sharding import PartitionSpec as P

EPSILON = 1e-05
LIMIT = 7.0
ALPHA = 1.702


def with_halo(x, sides, width):
    for axis, dim in sides:
        count, length = (lax.axis_size(axis), x.shape[dim])
        up = [(i, (i + 1) % count) for i in range(count - 1)]
        down = [(j, i) for i, j in up]
        last = lax.slice_in_dim(x, length - width, length, axis=dim)
        first = lax.slice_in_dim(x, 0, width, axis=dim)
        before = lax.ppermute(last, axis, up)
        after = lax.ppermute(first, axis, down)
        x = jnp.concatenate([before, x, after], axis=dim)
    return x


def clamped_unit(gate_pre, up_pre):
    gated = jnp.minimum(gate_pre, LIMIT)
    upward = jnp.clip(up_pre, -LIMIT, LIMIT)
    return (upward + 1.0) * gated * jax.nn.sigmoid(ALPHA * gated)


def block_ranks(chosen, block_rows, count):
    shaped = chosen.reshape(-1, block_rows)
    onehot = (shaped[:, :, None] == jnp.arange(count, dtype=jnp.int32)[None, None, :]).astype(
        jnp.int32
    )
    running = jnp.cumsum(onehot, axis=1) - 1
    return jnp.sum(running * onehot, axis=2).reshape(-1)


def local(
    conv_in,
    conv_pre,
    conv_post,
    taps,
    out_proj,
    stream,
    norm_gain,
    routes,
    route_weight,
    gate_w,
    up_w,
    down_w,
):
    product = conv_pre.astype(jnp.float32) * conv_in.astype(jnp.float32)
    padded = with_halo(product.astype(jnp.bfloat16), (("sp", 0),), 1).astype(product.dtype)
    convolved = taps[0] * padded[:-2] + taps[1] * padded[1:-1] + taps[2] * padded[2:]
    mixed = (conv_post.astype(jnp.float32) * convolved).astype(jnp.bfloat16)
    own_rows = stream.shape[0]
    width = stream.shape[1]
    regrouped = lax.all_to_all(mixed, "tp", split_axis=0, concat_axis=1, tiled=True)
    branch = jnp.dot(
        regrouped,
        lax.all_gather(out_proj, "tp", axis=0, tiled=True),
        preferred_element_type=jnp.float32,
    )
    resid = (stream.astype(jnp.float32) + branch).astype(jnp.bfloat16)
    resid_f = resid.astype(jnp.float32)
    scale = lax.rsqrt(jnp.mean(resid_f * resid_f, axis=-1, keepdims=True) + EPSILON)
    normed = (resid_f * scale * norm_gain).astype(jnp.bfloat16)
    group_rows, group_routes = (
        lax.all_gather(normed, "tp", axis=0, tiled=True),
        lax.all_gather(routes, "tp", axis=0, tiled=True),
    )
    top_count = routes.shape[1]
    quarters = lax.axis_size("tp")
    experts = gate_w.shape[0] * lax.axis_size("sp")
    capacity = max(2, own_rows * top_count * 4 // (3 * experts))
    group_flat = group_routes.reshape(-1)
    group_rank = block_ranks(group_flat, own_rows * top_count, experts)
    entry_ids = jnp.arange(group_flat.shape[0], dtype=jnp.int32)
    quarter_ids = entry_ids // (own_rows * top_count)
    targets = (group_flat * quarters + quarter_ids) * capacity + group_rank
    outgoing = jnp.zeros((experts * quarters * capacity, width), jnp.bfloat16)
    outgoing = outgoing.at[targets].set(group_rows[entry_ids // top_count])
    outgoing = outgoing.reshape(experts, quarters, capacity, width)
    arrived = lax.all_to_all(outgoing, "sp", split_axis=0, concat_axis=0, tiled=True)
    arrived_shape = arrived.shape
    rows_in = arrived.reshape(-1, width)
    gate_pre = jnp.dot(rows_in, gate_w[0], preferred_element_type=jnp.float32)
    up_pre = jnp.dot(rows_in, up_w[0], preferred_element_type=jnp.float32)
    active = clamped_unit(gate_pre, up_pre).astype(jnp.bfloat16)
    partial_value = jnp.dot(active, down_w[0], preferred_element_type=jnp.float32).reshape(
        arrived_shape
    )
    summed = lax.psum_scatter(
        partial_value.astype(jnp.bfloat16), "tp", scatter_dimension=1, tiled=True
    )
    returned = lax.all_to_all(summed, "sp", split_axis=0, concat_axis=0, tiled=True)
    back_rows = returned.reshape(-1, width)
    own_flat = routes.reshape(-1)
    own_rank = block_ranks(own_flat, own_rows * top_count, experts)
    picked = back_rows[own_flat * capacity + own_rank].reshape(own_rows, top_count, width)
    total = resid.astype(jnp.float32)
    for column in range(top_count):
        total = total + route_weight[:, column : column + 1] * picked[:, column].astype(jnp.float32)
    return total.astype(jnp.bfloat16)


def solution(mesh):
    placed = (
        P("sp", "tp"),
        P("sp", "tp"),
        P("sp", "tp"),
        P(None, "tp"),
        P("tp", None),
        P(("sp", "tp"), None),
        P(),
        P(("sp", "tp"), None),
        P(("sp", "tp"), None),
        P("sp", None, "tp"),
        P("sp", None, "tp"),
        P("sp", "tp", None),
    )
    return jax.shard_map(
        local, mesh=mesh, in_specs=placed, out_specs=P(("sp", "tp"), None), check_vma=False
    )
```

profile of v0, /device:TPU:0, one launch (start us, length us, event | category | flops | bytes accessed | tf_op | source)
XLA Modules:
  0.0 555.5 jit_solution(14085344026338815064)
XLA Ops:
  6.5 0.0 copy-start
  6.5 0.0 all-gather.4.cloned.1.call-start
  6.5 0.7 all-gather.4.cloned.1.call-update
  7.3 0.0 all-gather.6.cloned.1.call-start
  7.3 1.2 multiply_convert_fusion.2
  8.5 4.9 collective-permute-start
  13.4 1.3 collective-permute-start.1
  14.7 0.0 copy-done.7
  14.7 0.0 collective-permute-done
  14.7 4.1 collective-permute-done.1
  18.9 0.1 maximum_convert_fusion
  19.0 0.0 copy-done.4
  19.0 0.0 copy-start.3
  19.0 0.3 fusion.14
  19.3 14.6 %all_to_all.29 = bf16[4,192,256]{2,1,0:T(8,128)(2,1)S(1)} all-to-all(bf16[4,192,256]{2,1,0:T(8,128)(2,1)S(1)} %bitcast.92), channel_id=1, replica_groups=mesh['sp'=8,'tp'=4] {'tp'}, dimensions={0} | all-to-all | bytes 786432 | tf_op jit(solution)/shard_map/all_to_all | solution.py:59
  34.0 16.3 %all-gather.4.cloned.1.call-done = bf16[1024,2048]{1,0:T(8,128)(2,1)} async-done(((bf16[256,2048]{1,0:T(8,128)(2,1)}), bf16[1024,2048]{1,0:T(8,128)(2,1)}) %all-gather.4.cloned.1.call-update) | async-done | bytes 4194320 | tf_op jit(solution)/shard_map/all_gather | solution.py:62
  50.3 0.0 copy-done.3
  50.3 3.3 multiply_reduce_fusion
  53.7 0.0 copy-start.5
  53.7 1.1 copy-done.1
  54.8 0.0 copy-done.6
  54.8 1.1 multiply_convert_fusion.1
  55.9 0.0 all-gather.6.cloned.1.call-update
  55.9 0.0 all-reduce.3.cloned.1.call-start
  56.0 0.0 copy-done.5
  56.0 5.2 all-gather
  61.2 0.2 copy.42
  61.4 0.1 copy.45
  61.5 3.4 reduce-window.14
  64.9 0.1 slice.73
  65.0 0.1 copy.46
  65.1 0.1 copy.43
  65.2 0.1 fusion.16
  65.4 0.2 copy.41
  65.6 0.3 mul.153
  65.8 0.2 fusion.22
  66.1 18.5 %all-gather.6.cloned.1.call-done = bf16[768,2048]{1,0:T(8,128)(2,1)} async-done(((bf16[192,2048]{1,0:T(8,128)(2,1)}), bf16[768,2048]{1,0:T(8,128)(2,1)}) %all-gather.6.cloned.1.call-update) | async-done | bytes 3145744 | tf_op jit(solution)/shard_map/all_gather | solution.py:70
  84.6 31.7 %scatter_custom_fusion = bf16[2048,2048]{1,0:T(8,128)(2,1)} fusion(s32[1536]{0:T(1024)S(1)} %fusion.21, bf16[768,2048]{1,0:T(8,128)(2,1)} %all-gather.6.cloned.1.call-done, s32[2048]{0:T(1024)S(1)} %pad_clamp_fusion, bf16[]{:T(256)} %constant.25.clone.1), kind=kCustom, calls=%fused_computation.3 | custom fusion | bytes 8389120 | tf_op jit(solution)/shard_map/scatter | solution.py:83
  116.4 189.0 %all_to_all.30 = bf16[8,4,64,2048]{3,2,1,0:T(8,128)(2,1)S(1)} all-to-all(bf16[8,4,64,2048]{3,2,1,0:T(8,128)(2,1)} %bitcast.86), channel_id=1, replica_groups=mesh['sp'=8,'tp'=4] {'sp'}, dimensions={0} | all-to-all | bytes 16777216 | tf_op jit(solution)/shard_map/all_to_all | solution.py:85
  305.4 0.0 copy-done.9
  305.4 4.5 fusion.7
  309.9 0.0 copy-done.10
  309.9 5.7 %multiply_convert_fusion = bf16[2048,512]{1,0:T(8,128)(2,1)S(1)} fusion(f32[2048,512]{1,0:T(8,128)S(1)} %fusion.7, bf16[2048,2048]{1,0:T(8,128)(2,1)S(1)} %bitcast.88, bf16[1,2048,512]{2,1,0:T(8,128)(2,1)S(1)} %copy-done.10), kind=kOutput, calls=%fused_computation.6 | convolution fusion | flops 4305453056 | bytes 16777216 | tf_op jit(solution)/shard_map/dot_general | solution.py:88
  315.7 0.0 copy-done
  315.7 6.7 %convolution_convert_fusion = bf16[8,4,64,2048]{3,2,1,0:T(8,128)(2,1)} fusion(bf16[8,4,64,512]{3,2,1,0:T(8,128)(2,1)S(1)} %bitcast.103, bf16[1,512,2048]{2,1,0:T(8,128)(2,1)S(1)} %copy-done), kind=kOutput, calls=%fused_computation.5 | convolution fusion | flops 4299161600 | bytes 12582912 | tf_op jit(solution)/shard_map/dot_general | solution.py:91
  322.4 0.0 all-reduce.3.cloned.1.call-update
  322.4 0.6 copy-done.11
  323.1 0.6 dynamic-slice
  323.6 150.0 %all-reduce.3.cloned.1.call-done = bf16[8,4,64,2048]{3,2,1,0:T(8,128)(2,1)} async-done(((bf16[8,4,64,2048]{3,2,1,0:T(8,128)(2,1)}), bf16[8,4,64,2048]{3,2,1,0:T(8,128)(2,1)}) %all-reduce.3.cloned.1.call-update) | async-done | bytes 8388624
  473.6 3.9 constant_dynamic-slice_fusion
  477.5 5.6 %all-to-all-start.2 = ((bf16[8,1,64,2048]{3,2,1,0:T(8,128)(2,1)}), bf16[8,1,64,2048]{3,2,1,0:T(8,128)(2,1)}, u32[]{:S(2)}, u32[]{:S(2)}) async-start(bf16[8,1,64,2048]{3,2,1,0:T(8,128)(2,1)} %constant_dynamic-slice_fusion), calls=%async_computation.2 | async-start | bytes 4194304 | tf_op jit(solution)/shard_map/all_to_all | solution.py:97
  483.1 0.1 copy.49
  483.3 0.1 eq.60
  483.4 0.9 reduce-window.16
  484.3 0.2 slice_reduce_fusion
  484.6 0.1 copy.48
  484.7 0.1 mul.168
  484.8 0.1 fusion.18
  485.0 0.0 copy-done.8
  485.0 46.2 %all-to-all-done.2 = bf16[8,1,64,2048]{3,2,1,0:T(8,128)(2,1)} async-done(((bf16[8,1,64,2048]{3,2,1,0:T(8,128)(2,1)}), bf16[8,1,64,2048]{3,2,1,0:T(8,128)(2,1)}, u32[]{:S(2)}, u32[]{:S(2)}) %all-to-all-start.2) | async-done | bytes 2097184 | tf_op jit(solution)/shard_map/all_to_all | solution.py:97
  531.2 6.9 %gather_fusion = bf16[384,2048]{1,0:T(8,128)(2,1)} fusion(bf16[512,2048]{1,0:T(8,128)(2,1)} %bitcast.20, s32[1024]{0:T(1024)S(1)} %pad_clamp_fusion.1), kind=kCustom, calls=%fused_computation.1 | custom fusion | bytes 3147264 | tf_op jit(solution)/shard_map/gather | solution.py:101
  538.1 3.8 reshape.302
  541.9 4.4 fusion.28
  546.3 2.6 fusion.10
  (31 shorter events, 0.2 us)
Async XLA Ops:
  6.5 309.1 %copy-start = (bf16[1,512,2048]{2,1,0:T(8,128)(2,1)S(1)}, bf16[1,512,2048]{2,1,0:T(8,128)(2,1)}, u32[]{:S(2)}) copy-start(bf16[1,512,2048]{2,1,0:T(8,128)(2,1)} %param.23) | copy-start | bytes 6291460
  6.5 8.2 %copy-start.7 = (f32[3,256]{1,0:T(4,128)S(1)}, f32[3,256]{1,0:T(4,128)}, u32[]{:S(2)}) copy-start(f32[3,256]{1,0:T(4,128)} %param.15) | copy-start | bytes 9220
  6.5 12.4 %copy-start.4 = (bf16[768,256]{1,0:T(8,128)(2,1)S(1)}, bf16[768,256]{1,0:T(8,128)(2,1)}, u32[]{:S(2)}) copy-start(bf16[768,256]{1,0:T(8,128)(2,1)} %param.14) | copy-start | bytes 1179652
  6.5 43.8 %all-gather.4.cloned.1.call-start = ((), (), s32[]{:S(2)}) async-start(), calls=%async_computation.3 | async-start | bytes 5242880 | tf_op jit(solution)/shard_map/all_gather | solution.py:62
  7.3 77.4 %all-gather.6.cloned.1.call-start = ((), (), s32[]{:S(2)}) async-start(), calls=%async_computation.4 | async-start | bytes 3932160 | tf_op jit(solution)/shard_map/all_gather | solution.py:70
  8.5 6.2 %collective-permute-start = (bf16[1,256]{1,0:T(2,128)(2,1)S(1)}, bf16[1,256]{1,0:T(2,128)(2,1)S(1)}, u32[]{:S(2)}, u32[]{:S(2)}) collective-permute-start(bf16[1,256]{1,0:T(2,128)(2,1)S(1)} %get-tuple-element.7), channel_id=1, source_target_pairs={{0,4},{4,8},{8,12},{12,16},{16,20},{20,24},{24,28},{1,5},{5,9},{9,... | collective-permute-start | bytes 1544 | tf_op jit(solution)/shard_map/ppermute | solution.py:18
  13.4 5.5 collective-permute-start.1
  19.0 31.3 %copy-start.3 = (bf16[192,2048]{1,0:T(8,128)(2,1)S(1)}, bf16[192,2048]{1,0:T(8,128)(2,1)}, u32[]{:S(2)}) copy-start(bf16[192,2048]{1,0:T(8,128)(2,1)} %param.17) | copy-start | bytes 2359300
  50.3 4.5 copy-start.6
  53.7 1.2 copy-start.1
  53.7 2.3 copy-start.5
  55.9 417.7 %all-reduce.3.cloned.1.call-start = ((), (), s32[]{:S(2)}) async-start(), calls=%async_computation.5 | async-start | bytes 16777216
  116.4 189.0 %copy-start.9 = (bf16[1,2048,512]{2,1,0:T(8,128)(2,1)S(1)}, bf16[1,2048,512]{2,1,0:T(8,128)(2,1)}, u32[]{:S(2)}) copy-start(bf16[1,2048,512]{2,1,0:T(8,128)(2,1)} %param.22) | copy-start | bytes 6291460
  305.4 4.5 copy-start.10
  322.4 0.7 copy-start.11
  477.5 7.5 %copy-start.8 = (f32[192,2]{0,1:T(2,128)S(1)}, f32[192,2]{0,1:T(2,128)}, u32[]{:S(2)}) copy-start(f32[192,2]{0,1:T(2,128)} %param.20) | copy-start | bytes 4612
  477.5 53.7 %all-to-all-start.2 = ((bf16[8,1,64,2048]{3,2,1,0:T(8,128)(2,1)}), bf16[8,1,64,2048]{3,2,1,0:T(8,128)(2,1)}, u32[]{:S(2)}, u32[]{:S(2)}) async-start(bf16[8,1,64,2048]{3,2,1,0:T(8,128)(2,1)} %constant_dynamic-slice_fusion), calls=%async_computation.2 | async-start | bytes 4194304 | tf_op jit(solution)/shard_map/all_to_all | solution.py:97
  541.9 4.4 copy-start.2
Sparse Core Ops, SparseCore 0:
  8.9 41.3 all-gather.3
  56.1 28.5 all-gather.5
  322.6 151.0 all-reduce.2
where the time goes:
time: 556 us; the launch traced here: 555 us
  waiting for transfers between devices  236 us (42%)
  blocking collectives  209 us (38%)
  local copies, waits for them, and re-layouts  55 us (10%)
  matrix products  20.3 us (4%)
  between operations  13.4 us (2%)
  starting transfers between devices  11.9 us (2%)
  other arithmetic  10.1 us (2%)
    all_to_all x1, blocking collectives, local(): lax.all_to_all(outgoing, 'sp', split_axis=0, concat_axis=0, tiled=True)  189 us
    unnamed x4, waiting for transfers between devices  151 us
    all_to_all x1, waiting for transfers between devices, local(): lax.all_to_all(summed, 'sp', split_axis=0, concat_axis=0, tiled=True)  46.2 us
    scatter x1, local copies, waits for them, and re-layouts, local(): outgoing = outgoing.at[targets].set(group_rows[entry_ids // top_count])  31.7 us
    all_gather x1, waiting for transfers between devices, local(): lax.all_gather(normed, 'tp', axis=0, tiled=True)  18.5 us
    all_gather x1, waiting for transfers between devices, local(): lax.all_gather(out_proj, 'tp', axis=0, tiled=True)  16.3 us
    all_to_all x1, blocking collectives, local(): lax.all_to_all(mixed, 'tp', split_axis=0, concat_axis=1, tiled=True)  14.6 us
  transfers between devices with their start and end apart: 6, of which 5 were waited for; matrix products, arithmetic and copies ran while one was open for 2% of the time, Pallas kernels for 0%

commit v1 on v0

v1 whole, which is shorter than its diff:
```python
import functools

import jax
import jax.numpy as jnp
from jax import lax
from jax.experimental import pallas as pl
from jax.experimental.pallas import tpu as pltpu
from jax.sharding import PartitionSpec as P

EPSILON = 1e-05
LIMIT = 7.0
ALPHA = 1.702


def with_halo(x, sides, width):
    for axis, dim in sides:
        count, length = (lax.axis_size(axis), x.shape[dim])
        up = [(i, (i + 1) % count) for i in range(count - 1)]
        down = [(j, i) for i, j in up]
        last = lax.slice_in_dim(x, length - width, length, axis=dim)
        first = lax.slice_in_dim(x, 0, width, axis=dim)
        before = lax.ppermute(last, axis, up)
        after = lax.ppermute(first, axis, down)
        x = jnp.concatenate([before, x, after], axis=dim)
    return x

MESH = pl.DeviceIdType.MESH


def clamped_unit(gate_pre, up_pre):
    gated = jnp.minimum(gate_pre, LIMIT)
    upward = jnp.clip(up_pre, -LIMIT, LIMIT)
    return (upward + 1.0) * gated * jax.nn.sigmoid(ALPHA * gated)


def experts_kernel(
    n,
    group,
    disp,
    gate_w,
    up_w,
    down_w,
    out,
    rows,
    parts,
    partner_parts,
    chip_sum,
    peer_sum,
    final,
    gate_v,
    up_v,
    down_v,
    w_sem,
    own_sem,
    sp_send,
    sp_recv,
    pair_send,
    pair_recv,
    peer_send,
    peer_recv,
    fwd_send,
    fwd_recv,
    part_send,
    part_recv,
    sum_send,
    sum_recv,
    ret_send,
    ret_recv,
):
    steps = n // group
    me = lax.axis_index("sp")
    quarter = lax.axis_index("tp")
    y, c = quarter // 2, quarter % 2
    partner = {"tp": y * 2 + 1 - c}
    peer = {"tp": (1 - y) * 2 + c}

    def remote(source, target, send, recv, device):
        return pltpu.make_async_remote_copy(
            src_ref=source,
            dst_ref=target,
            send_sem=send,
            recv_sem=recv,
            device_id=device,
            device_id_type=MESH,
        )

    loads = [
        pltpu.make_async_copy(gate_w.at[0], gate_v, w_sem.at[0]),
        pltpu.make_async_copy(up_w.at[0], up_v, w_sem.at[1]),
        pltpu.make_async_copy(down_w.at[0], down_v, w_sem.at[2]),
    ]
    own_in = pltpu.make_async_copy(disp.at[me], rows.at[0, c, y, 0], own_sem.at[0])
    own_out = pltpu.make_async_copy(final.at[0, 0], out.at[me], own_sem.at[1])
    own_in.start()
    for load in loads:
        load.start()

    barrier = pltpu.get_barrier_semaphore()

    @pl.loop(1, n)
    def _(j):
        pl.semaphore_signal(barrier, inc=1, device_id={"sp": (me + j) % n}, device_id_type=MESH)

    pl.semaphore_signal(barrier, inc=1, device_id=partner, device_id_type=MESH)
    pl.semaphore_signal(barrier, inc=1, device_id=peer, device_id_type=MESH)
    pl.semaphore_wait(barrier, n + 1)

    def dispatch(j):
        to = (me + n - j) % n
        return remote(
            disp.at[to],
            rows.at[j // group, c, y, j % group],
            sp_send.at[j],
            sp_recv.at[j],
            {"sp": to},
        )

    def pair(t):
        block = rows.at[t, c, y]
        return remote(block, block, pair_send.at[t], pair_recv.at[t], partner)

    def across(t):
        block = rows.at[t, c, y]
        return remote(block, block, peer_send.at[t], peer_recv.at[t], peer)

    def forward(t):
        block = rows.at[t, c, 1 - y]
        return remote(block, block, fwd_send.at[t], fwd_recv.at[t], partner)

    def part(t):
        return remote(
            parts.at[t, 1 - c], partner_parts.at[t], part_send.at[t], part_recv.at[t], partner
        )

    def summed(t):
        return remote(chip_sum.at[t], peer_sum.at[t], sum_send.at[t], sum_recv.at[t], peer)

    def back(j):
        return remote(
            final.at[j // group, j % group],
            out.at[me],
            ret_send.at[j],
            ret_recv.at[j],
            {"sp": (me + j) % n},
        )

    @pl.loop(1, n)
    def _(j):
        dispatch(j).start()

    own_in.wait()
    for load in loads:
        load.wait()
    cap, width = rows.shape[-2:]
    count = 4 * group * cap

    def compute(t):
        x = rows[t].reshape(count, width)
        gate_pre = jnp.dot(x, gate_v[...], preferred_element_type=jnp.float32)
        up_pre = jnp.dot(x, up_v[...], preferred_element_type=jnp.float32)
        active = clamped_unit(gate_pre, up_pre).astype(jnp.bfloat16)
        tile = 512
        for at in range(0, width, tile):
            piece = jnp.dot(active, down_v[:, at : at + tile], preferred_element_type=jnp.float32)
            parts[t, :, :, :, :, at : at + tile] = piece.astype(jnp.bfloat16).reshape(
                2, 2, group, cap, tile
            )

    @pl.loop(0, steps + 4)
    def _(t):
        @pl.when(t < steps)
        def _():
            for g in range(group):
                j = t * group + g

                @pl.when(j > 0)
                def _():
                    dispatch(j).wait_recv()

            across(t).start()
            pair(t).start()

        @pl.when((t >= 1) & (t < steps + 1))
        def _():
            across(t - 1).wait_recv()
            forward(t - 1).start()

        @pl.when((t >= 2) & (t < steps + 2))
        def _():
            pair(t - 2).wait_recv()
            forward(t - 2).wait_recv()
            compute(t - 2)
            part(t - 2).start()

        @pl.when((t >= 3) & (t < steps + 3))
        def _():
            s = t - 3
            part(s).wait_recv()
            chip_sum[s] = (
                parts[s, c, 1 - y].astype(jnp.float32)
                + partner_parts[s, 1 - y].astype(jnp.float32)
            ).astype(jnp.bfloat16)
            summed(s).start()

        @pl.when(t >= 4)
        def _():
            s = t - 4
            summed(s).wait_recv()
            final[s] = (
                parts[s, c, y].astype(jnp.float32)
                + partner_parts[s, y].astype(jnp.float32)
                + peer_sum[s].astype(jnp.float32)
            ).astype(jnp.bfloat16)
            for g in range(group):
                j = s * group + g

                @pl.when(j > 0)
                def _():
                    back(j).start()

                @pl.when(j == 0)
                def _():
                    own_out.start()

    own_out.wait()

    @pl.loop(0, steps)
    def _(t):
        pair(t).wait_send()
        across(t).wait_send()
        forward(t).wait_send()
        part(t).wait_send()
        summed(t).wait_send()

    @pl.loop(1, n)
    def _(j):
        dispatch(j).wait_send()
        back(j).wait()


def run_experts(disp, gate_w, up_w, down_w):
    n, cap, width = disp.shape
    hidden = gate_w.shape[2]
    group = 1
    while n % (2 * group) == 0 and n // group > 8 and 4 * group * cap < 256:
        group *= 2
    steps = n // group
    kind = jnp.bfloat16
    hbm = pl.BlockSpec(memory_space=pltpu.HBM)
    dma = pltpu.SemaphoreType.DMA
    return pl.pallas_call(
        functools.partial(experts_kernel, n, group),
        out_shape=jax.ShapeDtypeStruct((n, cap, width), kind),
        in_specs=[hbm] * 4,
        out_specs=hbm,
        scratch_shapes=[
            pltpu.VMEM((steps, 2, 2, group, cap, width), kind),
            pltpu.VMEM((steps, 2, 2, group, cap, width), kind),
            pltpu.VMEM((steps, 2, group, cap, width), kind),
            pltpu.VMEM((steps, group, cap, width), kind),
            pltpu.VMEM((steps, group, cap, width), kind),
            pltpu.VMEM((steps, group, cap, width), kind),
            pltpu.VMEM((width, hidden), kind),
            pltpu.VMEM((width, hidden), kind),
            pltpu.VMEM((hidden, width), kind),
            dma((3,)),
            dma((2,)),
            dma((n,)),
            dma((n,)),
        ]
        + [dma((steps,))] * 10
        + [dma((n,))] * 2,
        compiler_params=pltpu.CompilerParams(
            collective_id=0, has_side_effects=True, vmem_limit_bytes=60 * 1024 * 1024
        ),
    )(disp, gate_w, up_w, down_w)


def local(
    conv_in,
    conv_pre,
    conv_post,
    taps,
    out_proj,
    stream,
    norm_gain,
    routes,
    route_weight,
    gate_w,
    up_w,
    down_w,
):
    product = conv_pre.astype(jnp.float32) * conv_in.astype(jnp.float32)
    padded = with_halo(product.astype(jnp.bfloat16), (("sp", 0),), 1).astype(product.dtype)
    convolved = taps[0] * padded[:-2] + taps[1] * padded[1:-1] + taps[2] * padded[2:]
    mixed = (conv_post.astype(jnp.float32) * convolved).astype(jnp.bfloat16)
    own_rows = stream.shape[0]
    width = stream.shape[1]
    regrouped = lax.all_to_all(mixed, "tp", split_axis=0, concat_axis=1, tiled=True)
    branch = jnp.dot(
        regrouped,
        lax.all_gather(out_proj, "tp", axis=0, tiled=True),
        preferred_element_type=jnp.float32,
    )
    resid = (stream.astype(jnp.float32) + branch).astype(jnp.bfloat16)
    resid_f = resid.astype(jnp.float32)
    scale = lax.rsqrt(jnp.mean(resid_f * resid_f, axis=-1, keepdims=True) + EPSILON)
    normed = (resid_f * scale * norm_gain).astype(jnp.bfloat16)
    top_count = routes.shape[1]
    experts = gate_w.shape[0] * lax.axis_size("sp")
    capacity = max(2, own_rows * top_count * 4 // (3 * experts))
    expert_ids = jnp.arange(experts, dtype=jnp.int32)
    chosen = routes[:, :, None] == expert_ids[None, None, :]
    named = jnp.any(chosen, axis=1)
    earlier = jnp.tri(own_rows, k=-1, dtype=jnp.bfloat16)
    ranks = jnp.dot(earlier, named.astype(jnp.bfloat16), preferred_element_type=jnp.float32)
    slots = expert_ids * capacity + ranks.astype(jnp.int32)
    slot_of = jnp.sum(jnp.where(chosen, slots[:, None, :], 0), axis=2)
    slot_ids = jnp.arange(experts * capacity, dtype=jnp.int32)
    onehots = [slot_of[:, k : k + 1] == slot_ids[None, :] for k in range(top_count)]
    spread = functools.reduce(jnp.logical_or, onehots).astype(jnp.bfloat16)
    disp = lax.dot_general(
        spread, normed, (((0,), (0,)), ((), ())), preferred_element_type=jnp.float32
    ).astype(jnp.bfloat16)
    back = run_experts(disp.reshape(experts, capacity, width), gate_w, up_w, down_w)
    back_rows = back.reshape(-1, width)
    total = resid.astype(jnp.float32)
    for column in range(top_count):
        picked = jnp.dot(
            onehots[column].astype(jnp.bfloat16), back_rows, preferred_element_type=jnp.float32
        )
        total = total + route_weight[:, column : column + 1] * picked
    return total.astype(jnp.bfloat16)


def solution(mesh):
    placed = (
        P("sp", "tp"),
        P("sp", "tp"),
        P("sp", "tp"),
        P(None, "tp"),
        P("tp", None),
        P(("sp", "tp"), None),
        P(),
        P(("sp", "tp"), None),
        P(("sp", "tp"), None),
        P("sp", None, "tp"),
        P("sp", None, "tp"),
        P("sp", "tp", None),
    )
    return jax.shard_map(
        local, mesh=mesh, in_specs=placed, out_specs=P(("sp", "tp"), None), check_vma=False
    )
```

time: 556 us -> 197 us (0.35)
  blocking collectives: 209 us -> 0 us
  waiting for transfers between devices: 236 us -> 31.2 us
  Pallas kernels: 0 us -> 126 us
  local copies, waits for them, and re-layouts: 55 us -> 0.08 us
  matrix products: 20.3 us -> 9.7 us
  other arithmetic: 10.1 us -> 2.39 us
    all_to_all x2 -> x0, blocking collectives: 204 us -> none  [the longest x1 189 us: local(): lax.all_to_all(outgoing, 'sp', split_axis=0, concat_axis=0, tiled=True)]
    unnamed x4 -> x1, waiting for transfers between devices: 151 us -> 0.71 us
    pallas_call x0 -> x1, Pallas kernels: none -> 126 us  [run_experts(): pl.pallas_call(functools.partial(experts_kernel, n, group), out_shape=jax...]
    all_to_all x1, waiting for transfers between devices: 46.2 us -> 12 us  [local(): lax.all_to_all(mixed, 'tp', split_axis=0, concat_axis=1, tiled=True)]
    scatter x1 -> x0, local copies, waits for them, and re-layouts: 31.7 us -> none  [local(): outgoing = outgoing.at[targets].set(group_rows[entry_ids // top_count])]
    all_gather x1 -> x0, waiting for transfers between devices: 18.5 us -> none  [local(): lax.all_gather(normed, 'tp', axis=0, tiled=True)]
    dot_general x3 -> x4, matrix products: 17 us -> 6.37 us  [the longest x2 3.91 us: local(): jnp.dot(onehots[column].astype(jnp.bfloat16), back_rows, preferred_elemen...]
    gather x1 -> x0, local copies, waits for them, and re-layouts: 6.91 us -> none  [local(): back_rows[own_flat * capacity + own_rank]]
  transfers between devices with their start and end apart: 6 -> 4, of which waited for: 5 -> 3; matrix products, arithmetic and copies ran while one was open for 2% -> 1% of each run, Pallas kernels for 0% -> 0%
where the time goes in v1:
time: 197 us; the launch traced here: 193 us
  Pallas kernels  126 us (64%)
  waiting for transfers between devices  31.2 us (16%)
  between operations  13.6 us (7%)
  starting transfers between devices  9.76 us (5%)
  matrix products  9.7 us (5%)
  other arithmetic  2.39 us (1%)
    pallas_call x1, Pallas kernels, run_experts(): pl.pallas_call(functools.partial(experts_kernel, n, group), out_shape=jax...  126 us
    all_gather x1, waiting for transfers between devices, local(): lax.all_gather(out_proj, 'tp', axis=0, tiled=True)  14.7 us
    all_to_all x1, waiting for transfers between devices, local(): lax.all_to_all(mixed, 'tp', split_axis=0, concat_axis=1, tiled=True)  12 us
    ppermute x1, starting transfers between devices, with_halo(): before = lax.ppermute(last, axis, up)  4.87 us
  transfers between devices with their start and end apart: 4, of which 3 were waited for; matrix products, arithmetic and copies ran while one was open for 1% of the time, Pallas kernels for 0%

profile of v1, /device:TPU:0, one launch (start us, length us, event | category | flops | bytes accessed | tf_op | source)
XLA Modules:
  0.0 193.0 jit_solution(4416605794128852341)
XLA Ops:
  6.5 0.0 copy-start.4
  6.5 0.0 copy-start.5
  6.5 0.0 copy-start.2
  6.5 0.0 all-gather.2.cloned.1.call-start
  6.5 0.7 all-gather.2.cloned.1.call-update
  7.3 1.2 multiply_convert_fusion.2
  8.5 4.9 %collective-permute-start = (bf16[1,256]{1,0:T(2,128)(2,1)S(1)}, bf16[1,256]{1,0:T(2,128)(2,1)S(1)}, u32[]{:S(2)}, u32[]{:S(2)}) collective-permute-start(bf16[1,256]{1,0:T(2,128)(2,1)S(1)} %get-tuple-element.5), channel_id=1, source_target_pairs={{0,4},{4,8},{8,12},{12,16},{16,20},{20,24},{24,28},{1,5},{5,9},{9,... | collective-permute-start | bytes 1544 | tf_op jit(solution)/shard_map/ppermute | solution.py:22
  13.4 1.3 collective-permute-start.1
  14.7 0.0 copy-done.4
  14.7 0.0 copy-done.5
  14.7 0.2 fusion.5
  15.0 0.0 collective-permute-done
  15.0 3.8 %collective-permute-done.1 = bf16[1,256]{1,0:T(2,128)(2,1)S(1)} collective-permute-done((bf16[1,256]{1,0:T(2,128)(2,1)S(1)}, bf16[1,256]{1,0:T(2,128)(2,1)S(1)}, u32[]{:S(2)}, u32[]{:S(2)}) %collective-permute-start.1) | collective-permute-done | bytes 544 | tf_op jit(solution)/shard_map/ppermute | solution.py:23
  18.8 0.1 maximum_convert_fusion
  18.9 0.0 copy-done.2
  18.9 0.0 copy-start.6
  18.9 1.0 fusion.8
  20.0 0.0 copy-start.1
  20.0 3.6 %all-to-all-start = ((bf16[4,192,256]{2,1,0:T(8,128)(2,1)}), bf16[4,192,256]{2,1,0:T(8,128)(2,1)S(1)}, u32[]{:S(2)}, u32[]{:S(2)}) async-start(bf16[4,192,256]{2,1,0:T(8,128)(2,1)} %bitcast.3), calls=%async_computation | async-start | bytes 786432 | tf_op jit(solution)/shard_map/all_to_all | solution.py:299
  23.6 0.0 copy-done.6
  23.6 12.0 %all-to-all-done = bf16[4,192,256]{2,1,0:T(8,128)(2,1)S(1)} async-done(((bf16[4,192,256]{2,1,0:T(8,128)(2,1)}), bf16[4,192,256]{2,1,0:T(8,128)(2,1)S(1)}, u32[]{:S(2)}, u32[]{:S(2)}) %all-to-all-start) | async-done | bytes 393248 | tf_op jit(solution)/shard_map/all_to_all | solution.py:299
  35.6 14.7 %all-gather.2.cloned.1.call-done = bf16[1024,2048]{1,0:T(8,128)(2,1)} async-done(((bf16[256,2048]{1,0:T(8,128)(2,1)}), bf16[1024,2048]{1,0:T(8,128)(2,1)}) %all-gather.2.cloned.1.call-update) | async-done | bytes 4194320 | tf_op jit(solution)/shard_map/all_gather | solution.py:302
  50.3 0.0 copy-done.1
  50.3 0.0 copy-start.3
  50.3 3.3 %multiply_reduce_fusion = (f32[192]{0:T(256)S(1)}, f32[192,2048]{1,0:T(8,128)S(1)}) fusion(bf16[192,1024]{1,0:T(8,128)(2,1)S(1)} %bitcast.22, bf16[1024,2048]{1,0:T(8,128)(2,1)} %all-gather.2.cloned.1.call-done, bf16[192,2048]{1,0:T(8,128)(2,1)S(1)} %copy-done.1), kind=kOutput, calls=%fused_computation.10 | convolution fusion | flops 807665472 | bytes 6947584 | tf_op jit(solution)/shard_map/dot_general | solution.py:300
  53.7 0.0 copy-done.3
  53.7 2.2 %convolution_convert_fusion = bf16[512,2048]{1,0:T(8,128)(2,1)} fusion(f32[192,2048]{1,0:T(8,128)S(1)} %get-tuple-element.15, f32[2048]{0:T(1024)S(1)} %copy-done.3, f32[192]{0:T(256)S(1)} %add_rsqrt_fusion, s32[192]{0:T(256)S(1)} %bitcast.25, s32[192]{0:T(256)S(1)} %bitcast.23), kind=kOutput, calls=%fused_computation | convolution fusion | flops 405176320 | bytes 3680512 | tf_op jit(solution)/shard_map/dot_general | solution.py:322
  55.9 126.3 %shard_map.118 = bf16[8,64,2048]{2,1,0:T(8,128)(2,1)} custom-call(bf16[8,64,2048]{2,1,0:T(8,128)(2,1)} %bitcast.20, bf16[1,2048,512]{2,1,0:T(8,128)(2,1)} %gate_w.1, bf16[1,2048,512]{2,1,0:T(8,128)(2,1)} %up_w.1, bf16[1,512,2048]{2,1,0:T(8,128)(2,1)} %down_w.1), custom_call_target="tpu_custom_call" | custom-call | tf_op jit(solution)/shard_map/pallas_call | solution.py:251
  182.2 0.0 copy-start
  182.2 2.4 %fusion.1 = f32[192,2048]{1,0:T(8,128)S(1)} fusion(f32[192,2048]{1,0:T(8,128)S(1)} %get-tuple-element.15, bf16[512,2048]{1,0:T(8,128)(2,1)} %bitcast.18, f32[192]{0:T(256)S(1)} %bitcast.30, s32[192]{0:T(256)S(1)} %bitcast.24), kind=kOutput, calls=%fused_computation.5 | convolution fusion | flops 403537920 | bytes 5244416 | tf_op jit(solution)/shard_map/dot_general | solution.py:329
  184.6 0.0 copy-done
  184.6 1.5 fusion.4
  (10 shorter events, 0.1 us)
Async XLA Ops:
  6.5 8.2 %copy-start.4 = (s32[192,2]{0,1:T(2,128)S(1)}, s32[192,2]{0,1:T(2,128)}, u32[]{:S(2)}) copy-start(s32[192,2]{0,1:T(2,128)} %param.19) | copy-start | bytes 4612
  6.5 8.2 %copy-start.5 = (f32[3,256]{1,0:T(4,128)S(1)}, f32[3,256]{1,0:T(4,128)}, u32[]{:S(2)}) copy-start(f32[3,256]{1,0:T(4,128)} %param.15) | copy-start | bytes 9220
  6.5 12.4 %copy-start.2 = (bf16[768,256]{1,0:T(8,128)(2,1)S(1)}, bf16[768,256]{1,0:T(8,128)(2,1)}, u32[]{:S(2)}) copy-start(bf16[768,256]{1,0:T(8,128)(2,1)} %param.14) | copy-start | bytes 1179652
  6.5 43.8 %all-gather.2.cloned.1.call-start = ((), (), s32[]{:S(2)}) async-start(), calls=%async_computation.1 | async-start | bytes 5242880 | tf_op jit(solution)/shard_map/all_gather | solution.py:302
  8.5 6.5 %collective-permute-start = (bf16[1,256]{1,0:T(2,128)(2,1)S(1)}, bf16[1,256]{1,0:T(2,128)(2,1)S(1)}, u32[]{:S(2)}, u32[]{:S(2)}) collective-permute-start(bf16[1,256]{1,0:T(2,128)(2,1)S(1)} %get-tuple-element.5), channel_id=1, source_target_pairs={{0,4},{4,8},{8,12},{12,16},{16,20},{20,24},{24,28},{1,5},{5,9},{9,... | collective-permute-start | bytes 1544 | tf_op jit(solution)/shard_map/ppermute | solution.py:22
  13.4 5.5 %collective-permute-start.1 = (bf16[1,256]{1,0:T(2,128)(2,1)S(1)}, bf16[1,256]{1,0:T(2,128)(2,1)S(1)}, u32[]{:S(2)}, u32[]{:S(2)}) collective-permute-start(bf16[1,256]{1,0:T(2,128)(2,1)S(1)} %get-tuple-element.6), channel_id=1, source_target_pairs={{4,0},{8,4},{12,8},{16,12},{20,16},{24,20},{28,24},{5,1},{9,5},{13... | collective-permute-start | bytes 1544 | tf_op jit(solution)/shard_map/ppermute | solution.py:23
  18.9 4.7 %copy-start.6 = (f32[192,2]{0,1:T(2,128)S(1)}, f32[192,2]{0,1:T(2,128)}, u32[]{:S(2)}) copy-start(f32[192,2]{0,1:T(2,128)} %param.20) | copy-start | bytes 4612
  20.0 30.3 %copy-start.1 = (bf16[192,2048]{1,0:T(8,128)(2,1)S(1)}, bf16[192,2048]{1,0:T(8,128)(2,1)}, u32[]{:S(2)}) copy-start(bf16[192,2048]{1,0:T(8,128)(2,1)} %param.17) | copy-start | bytes 2359300
  20.0 15.6 %all-to-all-start = ((bf16[4,192,256]{2,1,0:T(8,128)(2,1)}), bf16[4,192,256]{2,1,0:T(8,128)(2,1)S(1)}, u32[]{:S(2)}, u32[]{:S(2)}) async-start(bf16[4,192,256]{2,1,0:T(8,128)(2,1)} %bitcast.3), calls=%async_computation | async-start | bytes 786432 | tf_op jit(solution)/shard_map/all_to_all | solution.py:299
  50.3 3.3 %copy-start.3 = (f32[2048]{0:T(1024)S(1)}, f32[2048]{0:T(1024)}, u32[]{:S(2)}) copy-start(f32[2048]{0:T(1024)} %param.18) | copy-start | bytes 24580
  182.2 2.4 %copy-start = (bf16[8,64,2048]{2,1,0:T(8,128)(2,1)S(1)}, bf16[8,64,2048]{2,1,0:T(8,128)(2,1)}, u32[]{:S(2)}) copy-start(bf16[8,64,2048]{2,1,0:T(8,128)(2,1)} %shard_map.118) | copy-start | bytes 6291460
Sparse Core Ops, SparseCore 0:
  8.9 41.3 all-gather.1

commit v2 on v1

--- a/solution.py
+++ b/solution.py
@@ -10,19 +10,6 @@
 EPSILON = 1e-05
 LIMIT = 7.0
 ALPHA = 1.702
-
-
-def with_halo(x, sides, width):
-    for axis, dim in sides:
-        count, length = (lax.axis_size(axis), x.shape[dim])
-        up = [(i, (i + 1) % count) for i in range(count - 1)]
-        down = [(j, i) for i, j in up]
-        last = lax.slice_in_dim(x, length - width, length, axis=dim)
-        first = lax.slice_in_dim(x, 0, width, axis=dim)
-        before = lax.ppermute(last, axis, up)
-        after = lax.ppermute(first, axis, down)
-        x = jnp.concatenate([before, x, after], axis=dim)
-    return x
 
 MESH = pl.DeviceIdType.MESH
 
@@ -276,6 +263,265 @@
     )(disp, gate_w, up_w, down_w)
 
 
+CHUNKS = 4
+
+
+def mixer_kernel(
+    n,
+    conv_in,
+    conv_pre,
+    conv_post,
+    taps,
+    out_proj,
+    stream,
+    gain,
+    spread,
+    resid_out,
+    disp_out,
+    halo,
+    mixed,
+    regrouped,
+    w_pair,
+    w_peer,
+    w_far,
+    total,
+    halo_send,
+    halo_recv,
+    mix_send,
+    mix_recv,
+    pair_send,
+    pair_recv,
+    peer_send,
+    peer_recv,
+    swap_send,
+    swap_recv,
+    far_send,
+    far_recv,
+):
+    me = lax.axis_index("sp")
+    quarter = lax.axis_index("tp")
+    y, c = quarter // 2, quarter % 2
+    partner = {"tp": y * 2 + 1 - c}
+    peer = {"tp": (1 - y) * 2 + c}
+    half = me % 2
+    twin = {"sp": me + 1 - 2 * half}
+    length, channels = conv_in.shape
+    own_rows, width = stream.shape
+    edge = halo.shape[1]
+    depth = channels // 2 // CHUNKS
+
+    def remote(source, target, send, recv, device):
+        return pltpu.make_async_remote_copy(
+            src_ref=source,
+            dst_ref=target,
+            send_sem=send,
+            recv_sem=recv,
+            device_id=device,
+            device_id_type=MESH,
+        )
+
+    barrier = pltpu.get_barrier_semaphore()
+    for shift in (1, n - 1):
+        pl.semaphore_signal(
+            barrier, inc=1, device_id={"sp": (me + shift) % n}, device_id_type=MESH
+        )
+    for shift in (1, 2, 3):
+        pl.semaphore_signal(
+            barrier, inc=1, device_id={"tp": (quarter + shift) % 4}, device_id_type=MESH
+        )
+    pl.semaphore_wait(barrier, 5)
+
+    def up(k, source):
+        return remote(
+            source.at[length - edge : length],
+            halo.at[k],
+            halo_send.at[k],
+            halo_recv.at[k],
+            {"sp": (me + 1) % n},
+        )
+
+    def down(k, source):
+        return remote(
+            source.at[0:edge],
+            halo.at[2 + k],
+            halo_send.at[2 + k],
+            halo_recv.at[2 + k],
+            {"sp": (me + n - 1) % n},
+        )
+
+    def rows(h, k):
+        return pl.ds((h * CHUNKS + k) * depth, depth)
+
+    def whole():
+        return remote(out_proj, w_pair, pair_send.at[0], pair_recv.at[0], partner)
+
+    def across(k):
+        at = rows(half, k)
+        return remote(out_proj.at[at], w_peer.at[at], peer_send.at[k], peer_recv.at[k], peer)
+
+    def swap(k):
+        at = rows(half, k)
+        return remote(w_peer.at[at], w_peer.at[at], swap_send.at[k], swap_recv.at[k], twin)
+
+    def far(k, h, slot):
+        at = rows(h, k)
+        return remote(w_peer.at[at], w_far.at[at], far_send.at[slot], far_recv.at[slot], partner)
+
+    def send_mixed(shift):
+        return remote(
+            mixed.at[(quarter + shift) % 4],
+            regrouped.at[shift],
+            mix_send.at[shift],
+            mix_recv.at[shift],
+            {"tp": (quarter + shift) % 4},
+        )
+
+    @pl.when(me < n - 1)
+    def _():
+        up(0, conv_in).start()
+        up(1, conv_pre).start()
+
+    @pl.when(me > 0)
+    def _():
+        down(0, conv_in).start()
+        down(1, conv_pre).start()
+
+    for k in range(CHUNKS):
+        across(k).start()
+    whole().start()
+
+    @pl.when(me == 0)
+    def _():
+        halo[0:2] = jnp.zeros((2,) + halo.shape[1:], halo.dtype)
+
+    @pl.when(me == n - 1)
+    def _():
+        halo[2:4] = jnp.zeros((2,) + halo.shape[1:], halo.dtype)
+
+    @pl.when(me > 0)
+    def _():
+        up(0, conv_in).wait_recv()
+        up(1, conv_pre).wait_recv()
+
+    @pl.when(me < n - 1)
+    def _():
+        down(0, conv_in).wait_recv()
+        down(1, conv_pre).wait_recv()
+
+    product = conv_pre[...].astype(jnp.float32) * conv_in[...].astype(jnp.float32)
+    before_rows = halo[0].astype(jnp.float32) * halo[1].astype(jnp.float32)
+    after_rows = halo[2].astype(jnp.float32) * halo[3].astype(jnp.float32)
+    position = lax.broadcasted_iota(jnp.int32, product.shape, 0)
+    before = jnp.where(position == 0, before_rows[edge - 1 : edge], pltpu.roll(product, 1, 0))
+    after = jnp.where(
+        position == length - 1, after_rows[0:1], pltpu.roll(product, length - 1, 0)
+    )
+    convolved = taps[0:1] * before + taps[1:2] * product + taps[2:3] * after
+    value = (conv_post[...].astype(jnp.float32) * convolved).astype(jnp.bfloat16)
+    mixed[...] = value.reshape(mixed.shape)
+
+    for k in range(CHUNKS):
+        across(k).wait_recv()
+        swap(k).start()
+        far(k, half, k).start()
+        if k == 0:
+            for shift in (1, 2, 3):
+                send_mixed(shift).start()
+
+    total[...] = jnp.dot(mixed[quarter], out_proj[...], preferred_element_type=jnp.float32)
+    whole().wait_recv()
+
+    for k in range(CHUNKS):
+        swap(k).wait_recv()
+        far(k, 1 - half, CHUNKS + k).start()
+    for shift in (1, 2, 3):
+        send_mixed(shift).wait_recv()
+
+    def block(of):
+        return regrouped[(quarter + 4 - of) % 4]
+
+    total[...] += jnp.dot(
+        block(y * 2 + 1 - c), w_pair[...], preferred_element_type=jnp.float32
+    )
+    total[...] += jnp.dot(
+        block((1 - y) * 2 + c), w_peer[...], preferred_element_type=jnp.float32
+    )
+    for k in range(CHUNKS):
+        far(k, half, k).wait_recv()
+        far(k, 1 - half, CHUNKS + k).wait_recv()
+    branch = total[...] + jnp.dot(
+        block((1 - y) * 2 + 1 - c), w_far[...], preferred_element_type=jnp.float32
+    )
+    resid = (stream[...].astype(jnp.float32) + branch).astype(jnp.bfloat16)
+    resid_out[...] = resid
+    resid_f = resid.astype(jnp.float32)
+    scale = lax.rsqrt(jnp.mean(resid_f * resid_f, axis=-1, keepdims=True) + EPSILON)
+    normed = (resid_f * scale * gain[...]).astype(jnp.bfloat16)
+    tile = 512
+    for at in range(0, width, tile):
+        disp_out[:, at : at + tile] = jnp.dot(
+            spread[...], normed[:, at : at + tile], preferred_element_type=jnp.float32
+        ).astype(jnp.bfloat16)
+
+    @pl.when(me < n - 1)
+    def _():
+        up(0, conv_in).wait_send()
+        up(1, conv_pre).wait_send()
+
+    @pl.when(me > 0)
+    def _():
+        down(0, conv_in).wait_send()
+        down(1, conv_pre).wait_send()
+
+    whole().wait_send()
+    for k in range(CHUNKS):
+        across(k).wait_send()
+        swap(k).wait_send()
+        far(k, half, k).wait_send()
+        far(k, 1 - half, CHUNKS + k).wait_send()
+    for shift in (1, 2, 3):
+        send_mixed(shift).wait_send()
+
+
+def run_mixer(conv_in, conv_pre, conv_post, taps, out_proj, stream, gain, spread):
+    n = lax.axis_size("sp")
+    own_rows, width = stream.shape
+    channels = conv_in.shape[1]
+    slots = spread.shape[0]
+    kind = jnp.bfloat16
+    vmem = pl.BlockSpec(memory_space=pltpu.VMEM)
+    dma = pltpu.SemaphoreType.DMA
+    return pl.pallas_call(
+        functools.partial(mixer_kernel, n),
+        out_shape=(
+            jax.ShapeDtypeStruct((own_rows, width), kind),
+            jax.ShapeDtypeStruct((slots, width), kind),
+        ),
+        in_specs=[vmem] * 8,
+        out_specs=(vmem, vmem),
+        scratch_shapes=[
+            pltpu.VMEM((4, 16, channels), kind),
+            pltpu.VMEM((4, own_rows, channels), kind),
+            pltpu.VMEM((4, own_rows, channels), kind),
+            pltpu.VMEM((channels, width), kind),
+            pltpu.VMEM((channels, width), kind),
+            pltpu.VMEM((channels, width), kind),
+            pltpu.VMEM((own_rows, width), jnp.float32),
+            dma((4,)),
+            dma((4,)),
+            dma((4,)),
+            dma((4,)),
+            dma((1,)),
+            dma((1,)),
+        ]
+        + [dma((CHUNKS,))] * 4
+        + [dma((2 * CHUNKS,))] * 2,
+        compiler_params=pltpu.CompilerParams(
+            collective_id=1, has_side_effects=True, vmem_limit_bytes=40000 * 1024
+        ),
+    )(conv_in, conv_pre, conv_post, taps, out_proj, stream, gain, spread)
+
+
 def local(
     conv_in,
     conv_pre,
@@ -290,22 +536,8 @@
     up_w,
     down_w,
 ):
-    product = conv_pre.astype(jnp.float32) * conv_in.astype(jnp.float32)
-    padded = with_halo(product.astype(jnp.bfloat16), (("sp", 0),), 1).astype(product.dtype)
-    convolved = taps[0] * padded[:-2] + taps[1] * padded[1:-1] + taps[2] * padded[2:]
-    mixed = (conv_post.astype(jnp.float32) * convolved).astype(jnp.bfloat16)
     own_rows = stream.shape[0]
     width = stream.shape[1]
-    regrouped = lax.all_to_all(mixed, "tp", split_axis=0, concat_axis=1, tiled=True)
-    branch = jnp.dot(
-        regrouped,
-        lax.all_gather(out_proj, "tp", axis=0, tiled=True),
-        preferred_element_type=jnp.float32,
-    )
-    resid = (stream.astype(jnp.float32) + branch).astype(jnp.bfloat16)
-    resid_f = resid.astype(jnp.float32)
-    scale = lax.rsqrt(jnp.mean(resid_f * resid_f, axis=-1, keepdims=True) + EPSILON)
-    normed = (resid_f * scale * norm_gain).astype(jnp.bfloat16)
     top_count = routes.shape[1]
     experts = gate_w.shape[0] * lax.axis_size("sp")
     capacity = max(2, own_rows * top_count * 4 // (3 * experts))
@@ -318,10 +550,12 @@
     slot_of = jnp.sum(jnp.where(chosen, slots[:, None, :], 0), axis=2)
     slot_ids = jnp.arange(experts * capacity, dtype=jnp.int32)
     onehots = [slot_of[:, k : k + 1] == slot_ids[None, :] for k in range(top_count)]
-    spread = functools.reduce(jnp.logical_or, onehots).astype(jnp.bfloat16)
-    disp = lax.dot_general(
-        spread, normed, (((0,), (0,)), ((), ())), preferred_element_type=jnp.float32
+    spread = functools.reduce(
+        jnp.logical_or, [slot_ids[:, None] == slot_of[None, :, k] for k in range(top_count)]
     ).astype(jnp.bfloat16)
+    resid, disp = run_mixer(
+        conv_in, conv_pre, conv_post, taps, out_proj, stream, norm_gain[None, :], spread
+    )
     back = run_experts(disp.reshape(experts, capacity, width), gate_w, up_w, down_w)
     back_rows = back.reshape(-1, width)
     total = resid.astype(jnp.float32)

time: 197 us -> 168 us (0.85); the launches traced: 193 us -> 168 us
  waiting for transfers between devices: 31.2 us -> 0 us
  Pallas kernels: 126 us -> 154 us
  between operations: 13.6 us -> 0.09 us
  starting transfers between devices: 9.76 us -> 0 us
  local copies, waits for them, and re-layouts: 0.08 us -> 8.08 us
  matrix products: 9.7 us -> 4.13 us
    pallas_call x0 -> x1, Pallas kernels: none -> 24.5 us  [run_mixer(): pl.pallas_call(functools.partial(mixer_kernel, n), out_shape=(jax.ShapeDt...]
    all_gather x1 -> x0, waiting for transfers between devices: 14.7 us -> none  [local(): lax.all_gather(out_proj, 'tp', axis=0, tiled=True)]
    all_to_all x1 -> x0, waiting for transfers between devices: 12 us -> none  [local(): lax.all_to_all(mixed, 'tp', split_axis=0, concat_axis=1, tiled=True)]
    unnamed x14 -> x20, local copies, waits for them, and re-layouts: 0.03 us -> 8.07 us
    ppermute x2 -> x0, starting transfers between devices: 6.16 us -> none  [the longest x1 4.87 us: with_halo(): before = lax.ppermute(last, axis, up)]
    dot_general x2 -> x0, matrix products: 5.54 us -> none  [the longest x1 3.33 us: local(): jnp.dot(regrouped, lax.all_gather(out_proj, 'tp', axis=0, tiled=True), pr...]
    ppermute x2 -> x0, waiting for transfers between devices: 3.83 us -> none  [the longest x1 3.82 us: with_halo(): after = lax.ppermute(first, axis, down)]
    all_to_all x1 -> x0, starting transfers between devices: 3.59 us -> none  [local(): lax.all_to_all(mixed, 'tp', split_axis=0, concat_axis=1, tiled=True)]
  transfers between devices with their start and end apart: 4 -> 0, of which waited for: 3 -> 0; matrix products, arithmetic and copies ran while one was open for 1% -> 0% of each run, Pallas kernels for 0% -> 0%
where the time goes in v2:
time: 168 us
  Pallas kernels  154 us (92%)
  local copies, waits for them, and re-layouts  8.08 us (5%)
  matrix products  4.13 us (2%)
    pallas_call x1, Pallas kernels, run_experts(): pl.pallas_call(functools.partial(experts_kernel, n, group), out_shape=jax...  129 us
    pallas_call x1, Pallas kernels, run_mixer(): pl.pallas_call(functools.partial(mixer_kernel, n), out_shape=(jax.ShapeDt...  24.5 us
    unnamed x20, local copies, waits for them, and re-layouts  8.07 us
    dot_general x2, matrix products, local(): jnp.dot(onehots[column].astype(jnp.bfloat16), back_rows, preferred_elemen...  3.91 us

profile of v2, /device:TPU:0, one launch (start us, length us, event | category | flops | bytes accessed | tf_op | source)
XLA Modules:
  0.0 167.6 jit_solution(3912537635626042876)
XLA Ops:
  0.0 0.7 fusion.9
  0.7 0.2 fusion.3
  0.9 0.7 select_reduce_fusion
  1.7 0.1 fusion.5.spread
  1.8 0.0 copy-start.1
  1.8 1.2 copy-done.1
  3.0 0.0 copy-start.2
  3.0 1.1 copy-done.2
  4.1 0.0 copy-start.3
  4.1 1.0 copy-done.3
  5.1 0.0 copy-start.4
  5.1 1.0 copy-done.4
  6.1 0.0 copy-start.5
  6.1 1.0 copy-done.5
  7.1 0.0 copy-start.6
  7.1 0.7 copy-done.6
  7.8 0.0 copy-start.7
  7.8 0.7 copy-done.7
  8.5 24.5 %shard_map.118 = (bf16[192,2048]{1,0:T(8,128)(2,1)S(1)}, bf16[512,2048]{1,0:T(8,128)(2,1)S(1)}) custom-call(bf16[768,256]{1,0:T(8,128)(2,1)S(1)} %copy-done.3, bf16[768,256]{1,0:T(8,128)(2,1)S(1)} %copy-done.4, bf16[768,256]{1,0:T(8,128)(2,1)S(1)} %copy-done.5, f32[3,256]{1,0:T(4,128)S(1)} %copy-done.7, bf16[256,2048]{1,0:T(8,128)(2,1)S(1)} %copy-done.1, ...), custom_call_target="tpu_custom_call" | custom-call | tf_op jit(solution)/shard_map/pallas_call | solution.py:494
  33.1 0.0 copy-start
  33.1 1.3 copy-done
  34.4 0.0 copy-start.9
  34.4 129.2 %shard_map.119 = bf16[8,64,2048]{2,1,0:T(8,128)(2,1)} custom-call(bf16[8,64,2048]{2,1,0:T(8,128)(2,1)} %bitcast.10, bf16[1,2048,512]{2,1,0:T(8,128)(2,1)} %gate_w.1, bf16[1,2048,512]{2,1,0:T(8,128)(2,1)} %up_w.1, bf16[1,512,2048]{2,1,0:T(8,128)(2,1)} %down_w.1), custom_call_target="tpu_custom_call" | custom-call | tf_op jit(solution)/shard_map/pallas_call | solution.py:238
  163.6 0.0 copy-done.9
  163.6 0.0 copy-start.8
  163.6 2.4 %fusion.1 = f32[192,2048]{1,0:T(8,128)S(1)} fusion(bf16[512,2048]{1,0:T(8,128)(2,1)} %bitcast.12, bf16[192,2048]{1,0:T(8,128)(2,1)S(1)} %get-tuple-element.7, f32[192]{0:T(256)S(1)} %bitcast.19, s32[192]{0:T(256)S(1)} %bitcast.17), kind=kOutput, calls=%fused_computation.3 | convolution fusion | flops 403931136 | bytes 4457984 | tf_op jit(solution)/shard_map/dot_general | solution.py:563
  166.0 0.0 copy-done.8
  166.0 1.5 fusion.2
  (4 shorter events, 0.0 us)
Async XLA Ops:
  1.8 1.2 copy-start.1
  3.0 1.1 copy-start.2
  4.1 1.0 copy-start.3
  5.1 1.0 copy-start.4
  6.1 1.0 copy-start.5
  7.1 0.7 copy-start.6
  7.8 0.7 copy-start.7
  33.1 1.3 copy-start
  34.4 129.2 %copy-start.9 = (f32[192,2]{0,1:T(2,128)S(1)}, f32[192,2]{0,1:T(2,128)}, u32[]{:S(2)}) copy-start(f32[192,2]{0,1:T(2,128)} %param.20) | copy-start | bytes 4612
  163.6 2.4 %copy-start.8 = (bf16[8,64,2048]{2,1,0:T(8,128)(2,1)S(1)}, bf16[8,64,2048]{2,1,0:T(8,128)(2,1)}, u32[]{:S(2)}) copy-start(bf16[8,64,2048]{2,1,0:T(8,128)(2,1)} %shard_map.119) | copy-start | bytes 6291460
